TPU v7x, 32 devices: a whole 2x2x4 slice. The times are simulated.
32 devices in a mesh: sp: 4 (over y, x), dp: 8 (over z, core).
Axes of the slice: x: 2, y: 2, z: 4, core: 2. Of those that a mesh axis runs over, the one named last changes fastest.
Arguments:
- tokens: bfloat16 [8, 1280, 2048], P('dp', 'sp'), may hold values from -6 to 6
- up_weight: bfloat16 [2048, 2048], P('dp'), may hold values from -0.125 to 0.125
- gate_weight: bfloat16 [2048, 2048], P('dp'), may hold values from -0.125 to 0.125
- group_gain: float32 [16, 128], P('sp'), may hold values from 0.1 to 1.9
- mix_weight: bfloat16 [16, 1280, 1280], P('sp', 'dp'), may hold values from -0.15625 to 0.15625
- mix_bias: float32 [16, 1280], P('sp'), may hold values from 0.5 to 1.5
- out_gain: float32 [2048], replicated, may hold values from 0.1 to 1.9
- out_weight: bfloat16 [2048, 2048], P(None, 'dp'), may hold values from -0.125 to 0.125
Outputs:
- mixed_out: bfloat16 [8, 1280, 2048], P('dp', 'sp')
All inputs are finite; a program needn't handle non-finite values.
Results may differ from a plain program's by a relative error of at most 0.0072.
Values may be sent and summed in bfloat16 or wider, within the bound.
A program may use at most 128 MiB of HBM per device.

v0:
```python
import jax
import jax.numpy as jnp
from jax import lax
from jax.sharding import PartitionSpec as P

norm_eps = 1e-06


def body(tokens, up_weight, gate_weight, group_gain, mix_weight, mix_bias, out_gain, out_weight):
    sequences, per_device, model_width = tokens.shape
    groups_dev, group_dim = group_gain.shape
    groups = groups_dev * lax.axis_size("sp")
    mix_width = groups * group_dim
    flat_rows = tokens.reshape(sequences * per_device, model_width)
    full_mix = lax.all_gather(mix_weight, "dp", axis=1, tiled=True)
    block_len = full_mix.shape[1]
    lower = jnp.tril(jnp.ones((block_len, block_len), dtype=bool))
    masked_mix = jnp.where(lower[None], full_mix, jnp.zeros_like(full_mix))
    bias_cols = mix_bias.T

    def contract(shard_rows):
        return jnp.dot(flat_rows, shard_rows, preferred_element_type=jnp.float32)

    def by_group(product):
        return product.astype(jnp.bfloat16).reshape(sequences, per_device, groups, group_dim)

    up_proj = contract(lax.all_gather(up_weight, "dp", axis=0, tiled=True))
    gate_proj = contract(lax.all_gather(gate_weight, "dp", axis=0, tiled=True))
    up_heads = lax.all_to_all(by_group(up_proj), "sp", split_axis=2, concat_axis=1, tiled=True)
    gate_heads = lax.all_to_all(by_group(gate_proj), "sp", split_axis=2, concat_axis=1, tiled=True)
    members = up_heads.shape[0]
    seq_len = up_heads.shape[1]
    opened = jax.nn.gelu(up_heads.astype(jnp.float32))
    gate_act = jax.nn.gelu(gate_heads.astype(jnp.float32))
    center = jnp.mean(gate_act, axis=-1, keepdims=True)
    spread = jnp.mean(jnp.square(gate_act - center), axis=-1, keepdims=True)
    normal_v = ((gate_act - center) * lax.rsqrt(spread + norm_eps) * group_gain).astype(
        jnp.bfloat16
    )
    blocks = normal_v.reshape(members, seq_len // block_len, block_len, groups_dev, group_dim)
    mixed_sum = jnp.einsum(
        "gij,snjgc->snigc", masked_mix, blocks, preferred_element_type=jnp.float32
    )
    mixed_sum = mixed_sum + bias_cols[None, None, :, :, None]
    gated = (opened * mixed_sum.reshape(members, seq_len, groups_dev, group_dim)).astype(
        jnp.bfloat16
    )
    by_token = lax.all_to_all(gated, "sp", split_axis=1, concat_axis=2, tiled=True)
    gated_f = by_token.reshape(sequences * per_device, mix_width).astype(jnp.float32)
    scale = lax.rsqrt(jnp.mean(gated_f * gated_f, axis=-1, keepdims=True) + norm_eps)
    normed = (gated_f * scale * out_gain).astype(jnp.bfloat16)
    output = jnp.dot(
        normed,
        lax.all_gather(out_weight, "dp", axis=1, tiled=True),
        preferred_element_type=jnp.float32,
    )
    return output.astype(jnp.bfloat16).reshape(sequences, per_device, model_width)


def solution(mesh):
    return jax.shard_map(
        body,
        mesh=mesh,
        in_specs=(
            P("dp", "sp", None),
            P("dp", None),
            P("dp", None),
            P("sp", None),
            P("sp", "dp", None),
            P("sp", None),
            P(),
            P(None, "dp"),
        ),
        out_specs=P("dp", "sp", None),
        check_vma=False,
    )
```

profile of v0, /device:TPU:0, one launch (start us, length us, event | category | flops | bytes accessed | tf_op | source)
XLA Modules:
  0.0 393.9 jit_solution(9619464193229685776)
XLA Ops:
  6.5 0.7 all-gather.7.cloned.1.call-update
  7.3 0.7 all-gather.5.cloned.1.call-update
  8.1 0.7 all-gather.9.cloned.1.call-update
  8.8 0.5 all-gather.11.cloned.1.call-update
  9.3 84.4 %all-gather.7.cloned.1.call-done = bf16[2048,2048]{1,0:T(8,128)(2,1)} async-done(((bf16[256,2048]{1,0:T(8,128)(2,1)}), bf16[2048,2048]{1,0:T(8,128)(2,1)}) %all-gather.7.cloned.1.call-update) | async-done | bytes 8388624 | tf_op jit(solution)/shard_map/all_gather | solution.py:28
  93.7 6.3 %fusion.46 = bf16[40,8,16,128]{3,1,2,0:T(8,128)(2,1)S(1)} fusion(bf16[2048,2048]{1,0:T(8,128)(2,1)} %all-gather.7.cloned.1.call-done, bf16[1,320,2048]{2,1,0:T(8,128)(2,1)S(1)} %copy-done), kind=kOutput, calls=%fused_computation.48 | convolution fusion | flops 2685009920 | bytes 11010048 | tf_op jit(solution)/shard_map/dot_general | solution.py:22
  100.0 0.3 copy.80
  100.3 1.4 copy.69
  101.7 3.6 all-to-all-start.1
  105.4 1.7 iota_compare_fusion
  107.0 68.8 %all-gather.5.cloned.1.call-done = bf16[2048,2048]{1,0:T(8,128)(2,1)} async-done(((bf16[256,2048]{1,0:T(8,128)(2,1)}), bf16[2048,2048]{1,0:T(8,128)(2,1)}) %all-gather.5.cloned.1.call-update) | async-done | bytes 8388624 | tf_op jit(solution)/shard_map/all_gather | solution.py:27
  175.9 6.3 %fusion.45 = bf16[40,8,16,128]{3,1,2,0:T(8,128)(2,1)S(1)} fusion(bf16[2048,2048]{1,0:T(8,128)(2,1)} %all-gather.5.cloned.1.call-done, bf16[1,320,2048]{2,1,0:T(8,128)(2,1)S(1)} %copy-done), kind=kOutput, calls=%fused_computation.47 | convolution fusion | flops 2685009920 | bytes 11010048 | tf_op jit(solution)/shard_map/dot_general | solution.py:22
  182.1 0.3 copy.79
  182.4 1.4 copy.61
  183.8 3.8 all-to-all-start
  187.7 1.1 fusion.59
  188.8 1.9 multiply_reduce_fusion.1
  190.9 0.3 convert_bitcast_fusion.1
  191.2 1.7 copy.71
  192.9 11.6 %all-to-all-done = bf16[1,320,16,128]{3,1,0,2:T(8,128)(2,1)S(1)} async-done(((bf16[1,320,16,128]{3,1,0,2:T(8,128)(2,1)}), bf16[1,320,16,128]{3,1,0,2:T(8,128)(2,1)S(1)}, u32[]{:S(2)}, u32[]{:S(2)}) %all-to-all-start) | async-done | bytes 1310752 | tf_op jit(solution)/shard_map/all_to_all | solution.py:29
  204.5 0.3 convert_bitcast_fusion
  204.8 0.2 copy.63
  205.0 2.1 copy.68
  207.1 89.9 %all-gather.9.cloned.1.call-done = bf16[4,1280,1280]{2,1,0:T(8,128)(2,1)} async-done(((bf16[4,160,1280]{2,1,0:T(8,128)(2,1)}), bf16[4,1280,1280]{2,1,0:T(8,128)(2,1)}) %all-gather.9.cloned.1.call-update) | async-done | bytes 13107216 | tf_op jit(solution)/shard_map/all_gather | solution.py:15
  297.0 11.6 %fusion.16 = bf16[1,1280,4,128]{1,3,2,0:T(8,128)(2,1)S(1)} fusion(bf16[4,1280,1280]{2,1,0:T(8,128)(2,1)} %all-gather.9.cloned.1.call-done, pred[1280,1280]{1,0:T(8,128)(4,1)} %iota_compare_fusion, f32[1,1280,4,128]{1,3,2,0:T(8,128)} %copy.68, f32[1280,4,128]{2,0,1:T(8,128)} %bitcast.70, f32[1280,4]{0,1:T(4,128)S(1)} %bitcast.71, ...), kind=kOutput, calls=%fused_computation.12 | convolution fusion | flops 1699348480 | bytes 21362688 | tf_op jit(solution)/shard_map/gij,snjgc->snigc/dot_general | solution.py:41
  308.7 1.6 copy.75
  310.2 20.8 %all_to_all.12 = bf16[1,1280,4,128]{3,2,0,1:T(4,128)(2,1)S(1)} all-to-all(bf16[1,1280,4,128]{3,2,0,1:T(4,128)(2,1)S(1)} %copy.75), channel_id=1, replica_groups=mesh['sp'=4,'dp'=8] {'sp'}, dimensions={1} | all-to-all | bytes 2621440 | tf_op jit(solution)/shard_map/all_to_all | solution.py:48
  331.2 3.2 copy.77
  334.4 4.1 %reshape.191 = f32[320,2048]{1,0:T(8,128)} reshape(f32[1,320,4,4,128]{4,3,2,1,0:T(4,128)} %copy.77) | data formatting | bytes 5242880 | tf_op jit(solution)/shard_map/convert_element_type | solution.py:49
  338.6 0.3 multiply_reduce_fusion
  339.0 40.1 %all-gather.11.cloned.1.call-done = bf16[2048,2048]{1,0:T(8,128)(2,1)} async-done(((bf16[2048,256]{1,0:T(8,128)(2,1)}), bf16[2048,2048]{1,0:T(8,128)(2,1)}) %all-gather.11.cloned.1.call-update) | async-done | bytes 8388624 | tf_op jit(solution)/shard_map/all_gather | solution.py:54
  379.2 8.3 %fusion.44 = bf16[1,320,2048]{2,1,0:T(8,128)(2,1)} fusion(bf16[2048,2048]{1,0:T(8,128)(2,1)} %all-gather.11.cloned.1.call-done, f32[320,2048]{1,0:T(8,128)} %reshape.191, f32[2048]{0:T(1024)S(1)} %copy-done.3, f32[320]{0:T(512)S(1)} %add_rsqrt_fusion.1), kind=kOutput, calls=%fused_computation.46 | convolution fusion | flops 2686976000 | bytes 12330240 | tf_op jit(solution)/shard_map/dot_general | solution.py:52
  (25 shorter events, 0.6 us)
Async XLA Ops:
  6.5 87.2 %copy-start = (bf16[1,320,2048]{2,1,0:T(8,128)(2,1)S(1)}, bf16[1,320,2048]{2,1,0:T(8,128)(2,1)}, u32[]{:S(2)}) copy-start(bf16[1,320,2048]{2,1,0:T(8,128)(2,1)} %param.8) | copy-start | bytes 3932164
  6.5 87.2 %all-gather.7.cloned.1.call-start = ((), (), s32[]{:S(2)}) async-start(), calls=%async_computation.4 | async-start | bytes 9437184 | tf_op jit(solution)/shard_map/all_gather | solution.py:28
  7.3 168.6 %all-gather.5.cloned.1.call-start = ((), (), s32[]{:S(2)}) async-start(), calls=%async_computation.3 | async-start | bytes 9437184 | tf_op jit(solution)/shard_map/all_gather | solution.py:27
  8.0 289.0 %all-gather.9.cloned.1.call-start = ((), (), s32[]{:S(2)}) async-start(), calls=%async_computation.5 | async-start | bytes 14745600 | tf_op jit(solution)/shard_map/all_gather | solution.py:15
  8.7 370.4 %all-gather.11.cloned.1.call-start = ((), (), s32[]{:S(2)}) async-start(), calls=%async_computation.6 | async-start | bytes 9437184 | tf_op jit(solution)/shard_map/all_gather | solution.py:54
  101.7 82.1 %all-to-all-start.1 = ((bf16[1,320,16,128]{3,1,0,2:T(8,128)(2,1)}), bf16[1,320,16,128]{3,1,0,2:T(8,128)(2,1)S(1)}, u32[]{:S(2)}, u32[]{:S(2)}) async-start(bf16[1,320,16,128]{3,1,0,2:T(8,128)(2,1)} %copy.69), calls=%async_computation.1 | async-start | bytes 2621440 | tf_op jit(solution)/shard_map/all_to_all | solution.py:30
  183.8 20.7 %all-to-all-start = ((bf16[1,320,16,128]{3,1,0,2:T(8,128)(2,1)}), bf16[1,320,16,128]{3,1,0,2:T(8,128)(2,1)S(1)}, u32[]{:S(2)}, u32[]{:S(2)}) async-start(bf16[1,320,16,128]{3,1,0,2:T(8,128)(2,1)} %copy.61), calls=%async_computation | async-start | bytes 2621440 | tf_op jit(solution)/shard_map/all_to_all | solution.py:29
  204.9 92.1 %copy-start.2 = (f32[4,1280]{1,0:T(4,128)S(1)}, f32[4,1280]{1,0:T(4,128)}, u32[]{:S(2)}) copy-start(f32[4,1280]{1,0:T(4,128)} %param.13) | copy-start | bytes 61444
  205.0 92.1 %copy-start.4 = (f32[4,128]{1,0:T(4,128)S(1)}, f32[4,128]{1,0:T(4,128)}, u32[]{:S(2)}) copy-start(f32[4,128]{1,0:T(4,128)} %param.11) | copy-start | bytes 6148
  334.4 44.7 %copy-start.3 = (f32[2048]{0:T(1024)S(1)}, f32[2048]{0:T(1024)}, u32[]{:S(2)}) copy-start(f32[2048]{0:T(1024)} %param.14) | copy-start | bytes 24580
  379.2 8.3 %copy-start.1 = (bf16[1,320,2048]{2,1,0:T(8,128)(2,1)S(1)}, bf16[1,320,2048]{2,1,0:T(8,128)(2,1)}, u32[]{:S(2)}) copy-start(bf16[1,320,2048]{2,1,0:T(8,128)(2,1)} %param.8) | copy-start | bytes 3932164
Sparse Core Ops, SparseCore 0:
  8.9 84.7 all-gather.6
  95.3 80.5 all-gather.4
  177.5 119.4 all-gather.8
  298.5 80.6 all-gather.10
where the time goes:
time: 394 us
  waiting for transfers between devices  298 us (76%)
  matrix products  32.4 us (8%)
  blocking collectives  20.8 us (5%)
  local copies, waits for them, and re-layouts  16.6 us (4%)
  between operations  13.3 us (3%)
  starting transfers between devices  7.58 us (2%)
  other arithmetic  5.7 us (1%)
    all_gather x1, waiting for transfers between devices, body(): full_mix = lax.all_gather(mix_weight, 'dp', axis=1, tiled=True)  89.9 us
    all_gather x1, waiting for transfers between devices, body(): gate_proj = contract(lax.all_gather(gate_weight, 'dp', axis=0, tiled=True))  84.4 us
    all_gather x1, waiting for transfers between devices, body(): up_proj = contract(lax.all_gather(up_weight, 'dp', axis=0, tiled=True))  68.8 us
    all_gather x1, waiting for transfers between devices, body(): lax.all_gather(out_weight, 'dp', axis=1, tiled=True)  40.1 us
    all_to_all x1, blocking collectives, body(): lax.all_to_all(gated, 'sp', split_axis=1, concat_axis=2, tiled=True)  20.8 us
    dot_general x2, matrix products, contract(): return jnp.dot(flat_rows, shard_rows, preferred_element_type=jnp.float32)  12.5 us
    dot_general x1, matrix products, body(): jnp.einsum('gij,snjgc->snigc', masked_mix, blocks, preferred_element_type...  11.6 us
    all_to_all x1, waiting for transfers between devices, body(): lax.all_to_all(by_group(up_proj), 'sp', split_axis=2, concat_axis=1, tile...  11.6 us
  transfers between devices with their start and end apart: 6, of which 5 were waited for; matrix products, arithmetic and copies ran while one was open for 12% of the time, Pallas kernels for 0%

commit v1 on v0

v1 whole, which is shorter than its diff:
```python
import functools

import jax
import jax.numpy as jnp
from jax import lax
from jax.experimental import pallas as pl
from jax.experimental.pallas import tpu as pltpu
from jax.sharding import PartitionSpec as P

norm_eps = 1e-06
CORES = 2
MESH = pl.DeviceIdType.MESH


def gather_kernel(sp, zs, tok_ref, up_ref, gate_ref, mix_ref, outw_ref,
                  tok_full, ug_full, mix_full, out_full,
                  tok_v, ug_v, mix_v, outw_v,
                  load_sem, loc_sem, line_recv, up_send, down_send, part_send, part_recv,
                  tok_send, tok_recv, plane_send, plane_recv, pp_send, pp_recv):
    me = lax.axis_index("sp")
    dp = lax.axis_index("dp")
    z, c = dp // CORES, lax.rem(dp, CORES)
    groups, rows, block = mix_v.shape
    chans, ncol = outw_v.shape
    items = 2 + groups
    cut = pl.ds(pl.multiple_of(me * chans, 128), chans)

    loads = [
        pltpu.make_async_copy(tok_ref, tok_v, load_sem.at[0]),
        pltpu.make_async_copy(outw_ref.at[cut, :], outw_v, load_sem.at[1]),
        pltpu.make_async_copy(up_ref.at[:, cut], ug_v.at[0], load_sem.at[2]),
        pltpu.make_async_copy(gate_ref.at[:, cut], ug_v.at[1], load_sem.at[3]),
        pltpu.make_async_copy(mix_ref, mix_v, load_sem.at[4]),
    ]
    for load in loads:
        load.start()

    def at_line(zz):
        return {"dp": zz * CORES + c}

    partner = {"dp": z * CORES + (1 - c)}

    def peer(r):
        return {"sp": lax.rem(me + r, sp)}

    def width(o):
        return min(block, -(-((o + 1) * CORES * rows) // 128) * 128)

    def place(i, o, cc):
        if i == 0:
            return out_full.at[cc, me, :, pl.ds(o * ncol, ncol)]
        if i == 1:
            return ug_full.at[:, o * CORES + cc]
        return mix_full.at[i - 2, o * CORES + cc, :, pl.ds(0, width(o))]

    def own(i, zz):
        if i == 0:
            return outw_v
        if i == 1:
            return ug_v
        return mix_v.at[i - 2, :, pl.ds(0, width(zz))]

    def remote(src, dst, send, recv, device):
        return pltpu.make_async_remote_copy(
            src_ref=src, dst_ref=dst, send_sem=send, recv_sem=recv,
            device_id=device, device_id_type=MESH)

    def run(zz):
        sends, locs = [], []
        barrier = pltpu.get_barrier_semaphore()
        friends = [partner] + [peer(r) for r in range(1, sp)]
        if zz > 0:
            friends.append(at_line(zz - 1))
        if zz < zs - 1:
            friends.append(at_line(zz + 1))
        for friend in friends:
            pl.semaphore_signal(barrier, inc=1, device_id=friend, device_id_type=MESH)
        pl.semaphore_wait(barrier, len(friends))

        def push(copy):
            copy.start()
            sends.append(copy)

        def spread(i, o, src):
            dst = place(i, o, c)
            if o >= zz and zz > 0:
                push(remote(src, dst, down_send.at[i, o], line_recv.at[i, o], at_line(zz - 1)))
            if o <= zz and zz < zs - 1:
                push(remote(src, dst, up_send.at[i, o], line_recv.at[i, o], at_line(zz + 1)))
            push(remote(src, dst, part_send.at[i, o], part_recv.at[i, o], partner))

        def start_own(i):
            if i == 0:
                loads[1].wait()
            elif i == 1:
                loads[2].wait()
                loads[3].wait()
            elif i == 2:
                loads[4].wait()
            src = own(i, zz)
            spread(i, zz, src)
            copy = pltpu.make_async_copy(src, place(i, zz, c), loc_sem.at[i])
            copy.start()
            locs.append(copy)

        start_own(0)
        loads[0].wait()
        for r in range(1, sp):
            push(remote(tok_v, tok_full.at[me], tok_send.at[r], tok_recv.at[r], peer(r)))
        tok_copy = pltpu.make_async_copy(tok_v, tok_full.at[me], loc_sem.at[items])
        tok_copy.start()
        for i in range(items):
            if i + 1 < items:
                start_own(i + 1)
            for k in range(1, zs):
                for o in (zz + k, zz - k):
                    if 0 <= o < zs:
                        spot = place(i, o, c)
                        remote(spot, spot, up_send.at[i, o], line_recv.at[i, o], partner).wait_recv()
                        spread(i, o, spot)
            if i == 0:
                locs[0].wait()
                spot = out_full.at[c, me]
                for r in range(1, sp):
                    push(remote(spot, spot, plane_send.at[r], plane_recv.at[r], peer(r)))
        for r in range(1, sp):
            spot = out_full.at[c, lax.rem(me + sp - r, sp)]
            remote(spot, spot, plane_send.at[r], plane_recv.at[r], partner).wait_recv()
            push(remote(spot, spot, pp_send.at[r], pp_recv.at[r], partner))
        for i in range(items):
            for o in range(zs):
                spot = place(i, o, 1 - c)
                remote(spot, spot, part_send.at[i, o], part_recv.at[i, o], partner).wait_recv()
        for r in range(1, sp):
            source = lax.rem(me + sp - r, sp)
            spot = out_full.at[1 - c, source]
            remote(spot, spot, pp_send.at[r], pp_recv.at[r], partner).wait_recv()
            spot = tok_full.at[source]
            remote(spot, spot, tok_send.at[r], tok_recv.at[r], partner).wait_recv()
        for copy in sends:
            copy.wait_send()
        tok_copy.wait()
        for copy in locs[1:]:
            copy.wait()

    for zz in range(zs):
        pl.when(z == zz)(functools.partial(run, zz))


def gather_all(tokens, up_weight, gate_weight, mix_weight, out_weight, chans):
    sp, dps = lax.axis_size("sp"), lax.axis_size("dp")
    zs = dps // CORES
    groups, rows, block = mix_weight.shape
    depth = up_weight.shape[0]
    ncol = out_weight.shape[1]
    items = 2 + groups
    bf = jnp.bfloat16
    dma = pltpu.SemaphoreType.DMA
    return pl.pallas_call(
        functools.partial(gather_kernel, sp, zs),
        out_shape=(
            jax.ShapeDtypeStruct((sp,) + tokens.shape, bf),
            jax.ShapeDtypeStruct((2, dps, depth, chans), bf),
            jax.ShapeDtypeStruct((groups, dps, rows, block), bf),
            jax.ShapeDtypeStruct((CORES, sp, chans, zs * ncol), bf),
        ),
        in_specs=[pl.BlockSpec(memory_space=pl.ANY)] * 5,
        out_specs=[pl.BlockSpec(memory_space=pl.ANY)] * 4,
        scratch_shapes=[
            pltpu.VMEM(tokens.shape, bf),
            pltpu.VMEM((2, depth, chans), bf),
            pltpu.VMEM(mix_weight.shape, bf),
            pltpu.VMEM((chans, ncol), bf),
            dma((5,)),
            dma((items + 1,)),
            dma((items, zs)),
            dma((items, zs)),
            dma((items, zs)),
            dma((items, zs)),
            dma((items, zs)),
        ] + [dma((sp,))] * 6,
        compiler_params=pltpu.CompilerParams(collective_id=0, has_side_effects=True),
    )(tokens, up_weight, gate_weight, mix_weight, out_weight)


def body(tokens, up_weight, gate_weight, group_gain, mix_weight, mix_bias, out_gain, out_weight):
    sequences, per_device, model_width = tokens.shape
    groups_dev, group_dim = group_gain.shape
    sp = lax.axis_size("sp")
    chans = groups_dev * group_dim
    seq_len = per_device * sp
    tok_full, ug_full, mix_full, out_full = gather_all(
        tokens, up_weight, gate_weight, mix_weight, out_weight, chans
    )
    flat = jnp.moveaxis(tok_full, 0, 1).reshape(sequences * seq_len, model_width)
    ug = ug_full.reshape(2, model_width, chans)
    block_len = mix_full.shape[3]
    full_mix = mix_full.reshape(groups_dev, block_len, block_len)
    up_proj = jnp.dot(flat, ug[0], preferred_element_type=jnp.float32).astype(jnp.bfloat16)
    gate_proj = jnp.dot(flat, ug[1], preferred_element_type=jnp.float32).astype(jnp.bfloat16)
    up_heads = up_proj.reshape(sequences, seq_len, groups_dev, group_dim)
    gate_heads = gate_proj.reshape(sequences, seq_len, groups_dev, group_dim)
    opened = jax.nn.gelu(up_heads.astype(jnp.float32))
    gate_act = jax.nn.gelu(gate_heads.astype(jnp.float32))
    center = jnp.mean(gate_act, axis=-1, keepdims=True)
    spread = jnp.mean(jnp.square(gate_act - center), axis=-1, keepdims=True)
    normal_v = ((gate_act - center) * lax.rsqrt(spread + norm_eps) * group_gain).astype(
        jnp.bfloat16
    )
    lower = jnp.tril(jnp.ones((block_len, block_len), dtype=bool))
    masked_mix = jnp.where(lower[None], full_mix, jnp.zeros_like(full_mix))
    blocks = normal_v.reshape(sequences, seq_len // block_len, block_len, groups_dev, group_dim)
    mixed_sum = jnp.einsum(
        "gij,snjgc->snigc", masked_mix, blocks, preferred_element_type=jnp.float32
    )
    mixed_sum = mixed_sum + mix_bias.T[None, None, :, :, None]
    gated = (opened * mixed_sum.reshape(sequences, seq_len, groups_dev, group_dim)).astype(
        jnp.bfloat16
    ).reshape(sequences, seq_len, chans)
    by_token = lax.all_to_all(gated, "sp", split_axis=1, concat_axis=2, tiled=True)
    gated_f = by_token.reshape(sequences * per_device, sp * chans).astype(jnp.float32)
    scale = lax.rsqrt(jnp.mean(gated_f * gated_f, axis=-1, keepdims=True) + norm_eps)
    normed = (gated_f * scale * out_gain).astype(jnp.bfloat16)
    halves = out_full.reshape(CORES, sp * chans, -1)
    ncol = out_weight.shape[1]
    parts = [
        jnp.dot(normed, halves[h], preferred_element_type=jnp.float32)
        .astype(jnp.bfloat16)
        .reshape(sequences, per_device, -1, 1, ncol)
        for h in range(CORES)
    ]
    return jnp.concatenate(parts, axis=3).reshape(sequences, per_device, model_width)


def solution(mesh):
    return jax.shard_map(
        body,
        mesh=mesh,
        in_specs=(
            P("dp", "sp", None),
            P("dp", None),
            P("dp", None),
            P("sp", None),
            P("sp", "dp", None),
            P("sp", None),
            P(),
            P(None, "dp"),
        ),
        out_specs=P("dp", "sp", None),
        check_vma=False,
    )
```

time: 394 us -> 246 us (0.62)
  waiting for transfers between devices: 298 us -> 17.4 us
  Pallas kernels: 0 us -> 147 us
  blocking collectives: 20.8 us -> 0 us
  other arithmetic: 5.7 us -> 25.2 us
  between operations: 13.3 us -> 0.25 us
  local copies, waits for them, and re-layouts: 16.6 us -> 28.5 us
  matrix products: 32.4 us -> 23.7 us
    all_gather x4 -> x0, waiting for transfers between devices: 283 us -> none  [the longest x1 89.9 us: body(): full_mix = lax.all_gather(mix_weight, 'dp', axis=1, tiled=True)]
    pallas_call x0 -> x1, Pallas kernels: none -> 147 us  [gather_all(): pl.pallas_call(functools.partial(gather_kernel, sp, zs), out_shape=(jax.S...]
    all_to_all x1 -> x0, blocking collectives: 20.8 us -> none  [body(): lax.all_to_all(gated, 'sp', split_axis=1, concat_axis=2, tiled=True)]
    unnamed x0 -> x3, other arithmetic: none -> 9.49 us
    unnamed x12 -> x23, local copies, waits for them, and re-layouts: 0.62 us -> 7.62 us
    select_n x0 -> x1, other arithmetic: none -> 6.53 us  [body(): masked_mix = jnp.where(lower[None], full_mix, jnp.zeros_like(full_mix))]
    all_to_all x2 -> x1, waiting for transfers between devices: 11.6 us -> 17.4 us  [body(): lax.all_to_all(gated, 'sp', split_axis=1, concat_axis=2, tiled=True)]
    dot_general x3 -> x4, matrix products: 20.8 us -> 16.1 us  [the longest x1 7.44 us: body(): jnp.dot(flat, ug[0], preferred_element_type=jnp.float32)]
  transfers between devices with their start and end apart: 6 -> 1, of which waited for: 5 -> 1; matrix products, arithmetic and copies ran while one was open for 12% -> 0% of each run, Pallas kernels for 0% -> 0%
where the time goes in v1:
time: 246 us
  Pallas kernels  147 us (60%)
  local copies, waits for them, and re-layouts  28.5 us (12%)
  other arithmetic  25.2 us (10%)
  matrix products  23.7 us (10%)
  waiting for transfers between devices  17.4 us (7%)
  starting transfers between devices  4.29 us (2%)
    pallas_call x1, Pallas kernels, gather_all(): pl.pallas_call(functools.partial(gather_kernel, sp, zs), out_shape=(jax.S...  147 us
    all_to_all x1, waiting for transfers between devices, body(): lax.all_to_all(gated, 'sp', split_axis=1, concat_axis=2, tiled=True)  17.4 us
    convert_element_type x1, local copies, waits for them, and re-layouts, body(): (opened * mixed_sum.reshape(sequences, seq_len, groups_dev, group_dim)).a...  9.83 us
    unnamed x3, other arithmetic  9.49 us
    unnamed x23, local copies, waits for them, and re-layouts  7.62 us
    dot_general x1, matrix products, body(): jnp.einsum('gij,snjgc->snigc', masked_mix, blocks, preferred_element_type...  7.53 us
    dot_general x1, matrix products, body(): jnp.dot(flat, ug[0], preferred_element_type=jnp.float32)  7.44 us
    select_n x1, other arithmetic, body(): masked_mix = jnp.where(lower[None], full_mix, jnp.zeros_like(full_mix))  6.53 us
  transfers between devices with their start and end apart: 1, of which 1 were waited for; matrix products, arithmetic and copies ran while one was open for 0% of the time, Pallas kernels for 0%

profile of v1, /device:TPU:0, one launch (start us, length us, event | category | flops | bytes accessed | tf_op | source)
XLA Modules:
  0.0 246.0 jit_solution(15711226697537279602)
XLA Ops:
  0.0 0.5 iota_compare_fusion
  0.5 146.7 %shard_map.82 = (bf16[4,1,320,2048]{3,2,1,0:T(8,128)(2,1)}, bf16[2,8,256,512]{3,2,1,0:T(8,128)(2,1)}, bf16[4,8,160,1280]{3,2,1,0:T(8,128)(2,1)}, bf16[2,4,512,1024]{3,2,1,0:T(8,128)(2,1)}) custom-call(bf16[1,320,2048]{2,1,0:T(8,128)(2,1)} %tok_ref.1, bf16[256,2048]{1,0:T(8,128)(2,1)} %up_ref.1, bf16[256,2048]{1,0:T(8,128)(2,1)} %gate_ref.1, ...), custom_call_target="tpu_custom_call" | custom-call | tf_op jit(solution)/shard_map/pallas_call | solution.py:159
  147.2 0.0 copy-start.1
  147.2 4.1 %fusion.64 = (bf16[1,8,256,512]{3,2,1,0:T(8,128)(2,1)}, bf16[1,8,256,512]{3,2,1,0:T(8,128)(2,1)S(1)}) fusion(bf16[2,8,256,512]{3,2,1,0:T(8,128)(2,1)} %get-tuple-element.10), kind=kLoop, calls=%fused_computation.71 | loop fusion | bytes 8388608 | tf_op jit(solution)/shard_map/slice | solution.py:199
  151.4 0.0 slice-start.3
  151.4 3.2 %fusion.7 = f32[1280,512]{0,1:T(8,128)S(1)} fusion(bf16[1280,2048]{1,0:T(8,128)(2,1)S(1)} %bitcast.70, bf16[2048,512]{1,0:T(8,128)(2,1)S(1)} %bitcast.66), kind=kOutput, calls=%fused_computation.17 | convolution fusion | flops 2685665280 | bytes 9961472 | tf_op jit(solution)/shard_map/dot_general | solution.py:200
  154.6 0.9 fusion.57
  155.5 1.1 multiply_reduce_fusion.1
  156.6 0.0 copy-start.2
  156.7 0.0 copy-start.3
  156.7 6.5 %bitcast_select_fusion = bf16[4,1280,1280]{2,1,0:T(8,128)(2,1)} fusion(bf16[4,8,160,1280]{3,2,1,0:T(8,128)(2,1)S(1)} %bitcast.59, pred[1280,1280]{1,0:T(8,128)(4,1)S(1)} %iota_compare_fusion), kind=kLoop, calls=%fused_computation | loop fusion | flops 6553600 | bytes 27852800 | tf_op jit(solution)/shard_map/jit(_where)/select_n | solution.py:211
  163.2 7.5 %fusion.6 = f32[1,1,1280,4,128]{2,4,3,1,0:T(8,128)S(1)} fusion(bf16[4,1280,1280]{2,1,0:T(8,128)(2,1)} %bitcast_select_fusion, f32[1280,4,128]{0,2,1:T(8,128)S(1)} %bitcast.62, f32[1280,4]{0,1:T(4,128)S(1)} %bitcast.71, f32[4,128]{1,0:T(4,128)S(1)} %copy-done.3, f32[1280,4]{0,1:T(4,128)S(1)} %add_rsqrt_fusion, f32[1280,4]{0,1:T(4,128)S(1)} %broadcast_multiply_fusion), kind=kOutput, calls=%fused_computation.15 | convolution fusion | flops 1686241280 | bytes 18413568 | tf_op jit(solution)/shard_map/gij,snjgc->snigc/dot_general | solution.py:213
  170.7 2.1 copy.15
  172.9 7.4 %fusion.33 = bf16[1,1280,512]{2,1,0:T(8,128)(2,1)S(1)} fusion(f32[1280,512]{1,0:T(8,128)} %copy.15, bf16[1280,2048]{1,0:T(8,128)(2,1)} %bitcast.69, bf16[2048,512]{1,0:T(8,128)(2,1)} %bitcast.65), kind=kOutput, calls=%fused_computation.44 | convolution fusion | flops 2692218880 | bytes 11272192 | tf_op jit(solution)/shard_map/dot_general | solution.py:199
  180.3 9.8 %copy.26 = bf16[1,1280,512]{2,0,1:T(2,128)(2,1)S(1)} copy(bf16[1,1280,512]{2,1,0:T(8,128)(2,1)S(1)} %fusion.33) | data formatting | bytes 2621440 | tf_op jit(solution)/shard_map/convert_element_type | solution.py:217
  190.1 0.6 broadcast.235
  190.7 9.5 %reduce.4 = bf16[1280,512]{1,0:T(8,128)(2,1)} reduce(bf16[1280,1,512]{2,1,0:T(2,128)(2,1)S(1)} %bitcast.63, bf16[]{:T(256)} %broadcast.235), dimensions={1}, to_apply=%bitcast.55.reduce_sub_computation | reduce | bytes 2621442
  200.2 3.9 %reshape.230 = bf16[4,2,81920]{2,1,0:T(2,128)(2,1)} reshape(bf16[1280,512]{1,0:T(8,128)(2,1)} %reduce.4) | data formatting | bytes 2621440
  204.1 4.3 %all-to-all-start = ((bf16[4,2,81920]{2,1,0:T(2,128)(2,1)}), bf16[4,2,81920]{2,1,0:T(2,128)(2,1)}, u32[]{:S(2)}, u32[]{:S(2)}) async-start(bf16[4,2,81920]{2,1,0:T(2,128)(2,1)} %reshape.230), calls=%async_computation | async-start | bytes 2621440 | tf_op jit(solution)/shard_map/all_to_all | solution.py:220
  208.5 17.4 %all-to-all-done = bf16[4,2,81920]{2,1,0:T(2,128)(2,1)} async-done(((bf16[4,2,81920]{2,1,0:T(2,128)(2,1)}), bf16[4,2,81920]{2,1,0:T(2,128)(2,1)}, u32[]{:S(2)}, u32[]{:S(2)}) %all-to-all-start) | async-done | bytes 1310752 | tf_op jit(solution)/shard_map/all_to_all | solution.py:220
  225.8 3.1 %reshape.231 = bf16[1280,1,512]{2,1,0:T(2,128)(2,1)S(1)} reshape(bf16[4,2,81920]{2,1,0:T(2,128)(2,1)} %all-to-all-done) | data formatting | bytes 2621440
  228.9 0.0 slice-start.4
  228.9 2.7 %convert.3 = f32[1,4,320,512]{3,0,2,1:T(1,128)S(1)} convert(bf16[1,4,320,512]{3,0,2,1:T(2,128)(2,1)S(1)} %bitcast.56) | non-fusion elementwise | flops 655360 | bytes 3932160 | tf_op jit(solution)/shard_map/convert_element_type | solution.py:221
  231.6 3.1 %multiply_reduce_fusion = f32[320]{0:T(512)S(1)} fusion(bf16[1,4,320,512]{3,0,2,1:T(2,128)(2,1)S(1)} %bitcast.57), kind=kLoop, calls=%fused_computation.48 | loop fusion | flops 1965760 | bytes 1312000 | tf_op jit(solution)/shard_map/reduce_sum | solution.py:222
  234.8 3.9 %fusion.42 = bf16[320,1024]{1,0:T(8,128)(2,1)S(1)} fusion(bf16[2,4,512,1024]{3,2,1,0:T(8,128)(2,1)} %get-tuple-element.12, f32[1,4,320,512]{3,0,2,1:T(1,128)S(1)} %convert.3, f32[4,512]{1,0:T(4,128)S(1)} %mul.188, f32[320]{0:T(512)S(1)} %add_rsqrt_fusion.1), kind=kOutput, calls=%fused_computation.52 | convolution fusion | flops 1344471040 | bytes 7480576 | tf_op jit(solution)/shard_map/dot_general | solution.py:227
  238.7 0.0 slice-done.4
  238.7 1.6 fusion.45
  240.3 0.5 reshape.223
  240.8 0.5 reshape.221
  241.2 0.9 pad_maximum_fusion
  242.2 2.0 copy.14
  244.2 1.8 reshape.224
  (20 shorter events, 0.1 us)
Async XLA Ops:
  147.2 4.1 %copy-start.1 = (bf16[4,1,320,2048]{3,2,1,0:T(8,128)(2,1)S(1)}, bf16[4,1,320,2048]{3,2,1,0:T(8,128)(2,1)}, u32[]{:S(2)}) copy-start(bf16[4,1,320,2048]{3,2,1,0:T(8,128)(2,1)} %get-tuple-element.9) | copy-start | bytes 15728644
  151.3 5.3 %slice-start = ((s8[13107200]{0:T(1024)(128)(4,1)}), s8[4194304]{0:T(1024)(128)(4,1)S(1)}, s32[]{:S(2)}) async-start(s8[13107200]{0:T(1024)(128)(4,1)} %bitcast.58), calls=%async_computation.1 | async-start | bytes 8388608
  151.3 5.3 %slice-start.1 = ((s8[13107200]{0:T(1024)(128)(4,1)}), s8[4194304]{0:T(1024)(128)(4,1)S(1)}, s32[]{:S(2)}) async-start(s8[13107200]{0:T(1024)(128)(4,1)} %bitcast.58), calls=%async_computation.2 | async-start | bytes 8388608
  151.3 5.3 %slice-start.2 = ((s8[13107200]{0:T(1024)(128)(4,1)}), s8[4194304]{0:T(1024)(128)(4,1)S(1)}, s32[]{:S(2)}) async-start(s8[13107200]{0:T(1024)(128)(4,1)} %bitcast.58), calls=%async_computation.3 | async-start | bytes 8388608
  151.4 5.3 %slice-start.3 = ((s8[13107200]{0:T(1024)(128)(4,1)}), s8[524288]{0:T(1024)(128)(4,1)S(1)}, s32[]{:S(2)}) async-start(s8[13107200]{0:T(1024)(128)(4,1)} %bitcast.58), calls=%async_computation.4 | async-start | bytes 1048576
  156.6 6.6 %copy-start.2 = (f32[4,1280]{1,0:T(4,128)S(1)}, f32[4,1280]{1,0:T(4,128)}, u32[]{:S(2)}) copy-start(f32[4,1280]{1,0:T(4,128)} %param.13) | copy-start | bytes 61444
  156.7 6.6 %copy-start.3 = (f32[4,128]{1,0:T(4,128)S(1)}, f32[4,128]{1,0:T(4,128)}, u32[]{:S(2)}) copy-start(f32[4,128]{1,0:T(4,128)} %param.11) | copy-start | bytes 6148
  200.2 8.2 %copy-start = (f32[2048]{0:T(1024)S(1)}, f32[2048]{0:T(1024)}, u32[]{:S(2)}) copy-start(f32[2048]{0:T(1024)} %param.14) | copy-start | bytes 24580
  204.1 21.7 %all-to-all-start = ((bf16[4,2,81920]{2,1,0:T(2,128)(2,1)}), bf16[4,2,81920]{2,1,0:T(2,128)(2,1)}, u32[]{:S(2)}, u32[]{:S(2)}) async-start(bf16[4,2,81920]{2,1,0:T(2,128)(2,1)} %reshape.230), calls=%async_computation | async-start | bytes 2621440 | tf_op jit(solution)/shard_map/all_to_all | solution.py:220
  228.9 9.8 %slice-start.4 = ((s8[8388608]{0:T(1024)(128)(4,1)}), s8[4194304]{0:T(1024)(128)(4,1)S(1)}, s32[]{:S(2)}) async-start(s8[8388608]{0:T(1024)(128)(4,1)} %bitcast.67), calls=%async_computation.5 | async-start | bytes 8388608
  234.8 3.9 %slice-start.5 = ((s8[8388608]{0:T(1024)(128)(4,1)}), s8[4194304]{0:T(1024)(128)(4,1)S(1)}, s32[]{:S(2)}) async-start(s8[8388608]{0:T(1024)(128)(4,1)} %bitcast.67), calls=%async_computation.6 | async-start | bytes 8388608

commit v2 on v1

--- a/solution.py
+++ b/solution.py
@@ -183,6 +183,126 @@
     )(tokens, up_weight, gate_weight, mix_weight, out_weight)
 
 
+def mixer_kernel(flat_ref, ug_ref, gain_ref, mix_ref, bias_ref, out_ref, w_v, open_v, norm_v):
+    block, dim = out_ref.shape
+    step = 256 if block % 256 == 0 else block
+    w_v[:, :dim] = ug_ref[0]
+    w_v[:, dim:] = ug_ref[1]
+
+    @pl.loop(0, block // step)
+    def _(b):
+        rows = pl.ds(pl.multiple_of(b * step, step), step)
+        both = jnp.dot(flat_ref[rows, :], w_v[...], preferred_element_type=jnp.float32)
+        both = jax.nn.gelu(both.astype(jnp.bfloat16).astype(jnp.float32))
+        open_v[rows, :] = both[:, :dim]
+        act = both[:, dim:]
+        act = act - jnp.mean(act, axis=-1, keepdims=True)
+        spread = jnp.mean(act * act, axis=-1, keepdims=True)
+        norm_v[rows, :] = (act * lax.rsqrt(spread + norm_eps) * gain_ref[0]).astype(jnp.bfloat16)
+
+    keep = lax.broadcasted_iota(jnp.int32, (step, step), 0) >= lax.broadcasted_iota(
+        jnp.int32, (step, step), 1
+    )
+    for b in range(block // step):
+        lo, hi = b * step, (b + 1) * step
+        corner = jnp.where(keep, mix_ref[0, lo:hi, lo:hi].astype(jnp.float32), 0.0)
+        total = jnp.dot(
+            corner.astype(jnp.bfloat16), norm_v[lo:hi, :], preferred_element_type=jnp.float32
+        )
+        if b > 0:
+            total += jnp.dot(
+                mix_ref[0, lo:hi, :lo], norm_v[:lo, :], preferred_element_type=jnp.float32
+            )
+        total += jnp.broadcast_to(bias_ref[0, :, lo:hi], (dim, step)).T
+        out_ref[lo:hi, :] = (open_v[lo:hi, :] * total).astype(jnp.bfloat16)
+
+
+def mixer(flat, ug, group_gain, full_mix, mix_bias):
+    groups, block, _ = full_mix.shape
+    dim = group_gain.shape[1]
+    total, width = flat.shape
+    return pl.pallas_call(
+        mixer_kernel,
+        grid=(total // block, groups),
+        out_shape=jax.ShapeDtypeStruct((total, groups * dim), jnp.bfloat16),
+        in_specs=[
+            pl.BlockSpec((block, width), lambda n, g: (n, 0)),
+            pl.BlockSpec((2, width, dim), lambda n, g: (0, 0, g)),
+            pl.BlockSpec((1, 1, dim), lambda n, g: (g, 0, 0)),
+            pl.BlockSpec((1, block, block), lambda n, g: (g, 0, 0)),
+            pl.BlockSpec((1, 1, block), lambda n, g: (g, 0, 0)),
+        ],
+        out_specs=pl.BlockSpec((block, dim), lambda n, g: (n, g)),
+        scratch_shapes=[
+            pltpu.VMEM((width, 2 * dim), jnp.bfloat16),
+            pltpu.VMEM((block, dim), jnp.float32),
+            pltpu.VMEM((block, dim), jnp.bfloat16),
+        ],
+    )(flat, ug, group_gain[:, None, :], full_mix, mix_bias[:, None, :])
+
+
+def finish_kernel(sp, gated_ref, gain_ref, w_ref, out_ref, held, normed, send_sem, recv_sem):
+    me = lax.axis_index("sp")
+    rows, chans = held.shape[1:]
+    ncol = out_ref.shape[2]
+    barrier = pltpu.get_barrier_semaphore()
+    for r in range(1, sp):
+        pl.semaphore_signal(
+            barrier, inc=1, device_id={"sp": lax.rem(me + r, sp)}, device_id_type=MESH
+        )
+    pl.semaphore_wait(barrier, sp - 1)
+    copies = []
+    for r in range(1, sp):
+        to = lax.rem(me + r, sp)
+        copies.append(
+            pltpu.make_async_remote_copy(
+                src_ref=gated_ref.at[to], dst_ref=held.at[me],
+                send_sem=send_sem.at[r], recv_sem=recv_sem.at[r],
+                device_id={"sp": to}, device_id_type=MESH)
+        )
+    for copy in copies:
+        copy.start()
+    held[me] = gated_ref[me]
+    for copy in copies:
+        copy.wait()
+    squares = jnp.zeros((rows, 1), jnp.float32)
+    for s in range(sp):
+        part = held[s].astype(jnp.float32)
+        squares += jnp.sum(part * part, axis=-1, keepdims=True)
+    scale = lax.rsqrt(squares / (sp * chans) + norm_eps)
+    for s in range(sp):
+        cols = slice(s * chans, (s + 1) * chans)
+        normed[:, cols] = (held[s].astype(jnp.float32) * scale * gain_ref[:, cols]).astype(
+            jnp.bfloat16
+        )
+
+    @pl.loop(0, w_ref.shape[2] // ncol)
+    def _(o):
+        for h in range(CORES):
+            cols = pl.ds(pl.multiple_of(o * ncol, ncol), ncol)
+            out_ref[o * CORES + h] = jnp.dot(
+                normed[...], w_ref[h, :, cols], preferred_element_type=jnp.float32
+            ).astype(jnp.bfloat16)
+
+
+def finish(gated, out_gain, halves, ncol):
+    sp, rows, chans = gated.shape
+    vmem = pl.BlockSpec(memory_space=pltpu.VMEM)
+    return pl.pallas_call(
+        functools.partial(finish_kernel, sp),
+        out_shape=jax.ShapeDtypeStruct((CORES * halves.shape[2] // ncol, rows, ncol), jnp.bfloat16),
+        in_specs=[vmem] * 3,
+        out_specs=vmem,
+        scratch_shapes=[
+            pltpu.VMEM(gated.shape, jnp.bfloat16),
+            pltpu.VMEM((rows, sp * chans), jnp.bfloat16),
+            pltpu.SemaphoreType.DMA((sp,)),
+            pltpu.SemaphoreType.DMA((sp,)),
+        ],
+        compiler_params=pltpu.CompilerParams(collective_id=1, has_side_effects=True),
+    )(gated, out_gain[None, :], halves)
+
+
 def body(tokens, up_weight, gate_weight, group_gain, mix_weight, mix_bias, out_gain, out_weight):
     sequences, per_device, model_width = tokens.shape
     groups_dev, group_dim = group_gain.shape
@@ -196,40 +316,12 @@
     ug = ug_full.reshape(2, model_width, chans)
     block_len = mix_full.shape[3]
     full_mix = mix_full.reshape(groups_dev, block_len, block_len)
-    up_proj = jnp.dot(flat, ug[0], preferred_element_type=jnp.float32).astype(jnp.bfloat16)
-    gate_proj = jnp.dot(flat, ug[1], preferred_element_type=jnp.float32).astype(jnp.bfloat16)
-    up_heads = up_proj.reshape(sequences, seq_len, groups_dev, group_dim)
-    gate_heads = gate_proj.reshape(sequences, seq_len, groups_dev, group_dim)
-    opened = jax.nn.gelu(up_heads.astype(jnp.float32))
-    gate_act = jax.nn.gelu(gate_heads.astype(jnp.float32))
-    center = jnp.mean(gate_act, axis=-1, keepdims=True)
-    spread = jnp.mean(jnp.square(gate_act - center), axis=-1, keepdims=True)
-    normal_v = ((gate_act - center) * lax.rsqrt(spread + norm_eps) * group_gain).astype(
-        jnp.bfloat16
-    )
-    lower = jnp.tril(jnp.ones((block_len, block_len), dtype=bool))
-    masked_mix = jnp.where(lower[None], full_mix, jnp.zeros_like(full_mix))
-    blocks = normal_v.reshape(sequences, seq_len // block_len, block_len, groups_dev, group_dim)
-    mixed_sum = jnp.einsum(
-        "gij,snjgc->snigc", masked_mix, blocks, preferred_element_type=jnp.float32
-    )
-    mixed_sum = mixed_sum + mix_bias.T[None, None, :, :, None]
-    gated = (opened * mixed_sum.reshape(sequences, seq_len, groups_dev, group_dim)).astype(
-        jnp.bfloat16
-    ).reshape(sequences, seq_len, chans)
-    by_token = lax.all_to_all(gated, "sp", split_axis=1, concat_axis=2, tiled=True)
-    gated_f = by_token.reshape(sequences * per_device, sp * chans).astype(jnp.float32)
-    scale = lax.rsqrt(jnp.mean(gated_f * gated_f, axis=-1, keepdims=True) + norm_eps)
-    normed = (gated_f * scale * out_gain).astype(jnp.bfloat16)
+    gated = mixer(flat, ug, group_gain, full_mix, mix_bias)
+    gated = jnp.moveaxis(gated.reshape(sequences, sp, per_device, chans), 1, 0)
+    gated = gated.reshape(sp, sequences * per_device, chans)
     halves = out_full.reshape(CORES, sp * chans, -1)
-    ncol = out_weight.shape[1]
-    parts = [
-        jnp.dot(normed, halves[h], preferred_element_type=jnp.float32)
-        .astype(jnp.bfloat16)
-        .reshape(sequences, per_device, -1, 1, ncol)
-        for h in range(CORES)
-    ]
-    return jnp.concatenate(parts, axis=3).reshape(sequences, per_device, model_width)
+    output = finish(gated, out_gain, halves, out_weight.shape[1])
+    return jnp.moveaxis(output, 0, 1).reshape(sequences, per_device, model_width)
 
 
 def solution(mesh):

time: 246 us -> 199 us (0.81)
  Pallas kernels: 147 us -> 194 us
  other arithmetic: 25.2 us -> 0 us
  matrix products: 23.7 us -> 0 us
  local copies, waits for them, and re-layouts: 28.5 us -> 4.86 us
  waiting for transfers between devices: 17.4 us -> 0 us
  starting transfers between devices: 4.29 us -> 0 us
    pallas_call x0 -> x2, Pallas kernels: none -> 47.7 us  [the longest x1 26.3 us: finish(): pl.pallas_call(functools.partial(finish_kernel, sp), out_shape=jax.ShapeD...]
    dot_general x5 -> x0, matrix products: 23.7 us -> none  [the longest x1 7.53 us: body(): jnp.einsum('gij,snjgc->snigc', masked_mix, blocks, preferred_element_type...]
    all_to_all x1 -> x0, waiting for transfers between devices: 17.4 us -> none  [body(): lax.all_to_all(gated, 'sp', split_axis=1, concat_axis=2, tiled=True)]
    convert_element_type x1 -> x0, local copies, waits for them, and re-layouts: 9.83 us -> none  [body(): (opened * mixed_sum.reshape(sequences, seq_len, groups_dev, group_dim)).a...]
    unnamed x3 -> x0, other arithmetic: 9.49 us -> none
    unnamed x23 -> x0, local copies, waits for them, and re-layouts: 7.62 us -> none
    select_n x1 -> x0, other arithmetic: 6.53 us -> none  [body(): masked_mix = jnp.where(lower[None], full_mix, jnp.zeros_like(full_mix))]
    reduce_sum x3 -> x0, other arithmetic: 5.08 us -> none  [the longest x1 3.13 us: body(): jnp.mean(gated_f * gated_f, axis=-1, keepdims=True) + norm_eps]
  transfers between devices with their start and end apart: 1 -> 0, of which waited for: 1 -> 0; matrix products, arithmetic and copies ran while one was open for 0% -> 0% of each run, Pallas kernels for 0% -> 0%
where the time goes in v2:
time: 199 us
  Pallas kernels  194 us (97%)
  local copies, waits for them, and re-layouts  4.86 us (2%)
    pallas_call x1, Pallas kernels, gather_all(): pl.pallas_call(functools.partial(gather_kernel, sp, zs), out_shape=(jax.S...  147 us
    pallas_call x1, Pallas kernels, finish(): pl.pallas_call(functools.partial(finish_kernel, sp), out_shape=jax.ShapeD...  26.3 us
    pallas_call x1, Pallas kernels, mixer(): pl.pallas_call(mixer_kernel, grid=(total // block, groups), out_shape=jax...  21.4 us

profile of v2, /device:TPU:0, one launch (start us, length us, event | category | flops | bytes accessed | tf_op | source)
XLA Modules:
  0.0 199.3 jit_solution(16879862992149871621)
XLA Ops:
  0.0 1.3 broadcast_in_dim.10.bias_ref
  1.3 146.7 %shard_map.82 = (bf16[4,1,320,2048]{3,2,1,0:T(8,128)(2,1)}, bf16[2,8,256,512]{3,2,1,0:T(8,128)(2,1)}, bf16[4,8,160,1280]{3,2,1,0:T(8,128)(2,1)}, bf16[2,4,512,1024]{3,2,1,0:T(8,128)(2,1)}) custom-call(bf16[1,320,2048]{2,1,0:T(8,128)(2,1)} %tok_ref.1, bf16[256,2048]{1,0:T(8,128)(2,1)} %up_ref.1, bf16[256,2048]{1,0:T(8,128)(2,1)} %gate_ref.1, ...), custom_call_target="tpu_custom_call" | custom-call | tf_op jit(solution)/shard_map/pallas_call | solution.py:159
  148.0 21.4 %shard_map.83 = bf16[1280,512]{1,0:T(8,128)(2,1)} custom-call(bf16[1280,2048]{1,0:T(8,128)(2,1)} %bitcast.12, bf16[2,2048,512]{2,1,0:T(8,128)(2,1)} %bitcast.13, f32[4,1,128]{2,1,0:T(1,128)} %bitcast.15, bf16[4,1280,1280]{2,1,0:T(8,128)(2,1)} %bitcast.8, f32[4,1,1280]{2,1,0:T(1,128)} %broadcast_in_dim.10.bias_ref), custom_call_target="tpu_custom_call" | custom-call | tf_op jit(solution)/shard_map/pallas_call | solution.py:224
  169.4 26.3 %shard_map.84 = bf16[8,320,256]{2,1,0:T(8,128)(2,1)} custom-call(bf16[4,320,512]{2,1,0:T(8,128)(2,1)} %bitcast.10, f32[1,2048]{1,0:T(1,128)} %bitcast.14, bf16[2,2048,1024]{2,1,0:T(8,128)(2,1)} %bitcast.9), custom_call_target="tpu_custom_call" | custom-call | tf_op jit(solution)/shard_map/pallas_call | solution.py:291
  195.7 2.0 %copy.9 = bf16[320,8,256]{2,1,0:T(8,128)(2,1)S(1)} copy(bf16[320,8,256]{2,0,1:T(8,128)(2,1)} %bitcast.11) | data formatting | bytes 2621440 | tf_op jit(solution)/shard_map/transpose | solution.py:324
  197.8 1.5 reshape.15
